TPU v7x, 256 devices: a whole 4x4x8 slice. The times are simulated.
256 devices in a mesh: kv: 16 (over y, x), tp: 16 (over z, core).
Axes of the slice: x: 4, y: 4, z: 8, core: 2. Of those that a mesh axis runs over, the one named last changes fastest.
Arguments:
- tokens: bfloat16 [128, 4096], P(None, ('kv', 'tp')), may hold values from -41 to 41
- lengths: int32 [128], P('kv'), may hold values from 1 to 8192, 262144 in all
- retention_state: float32 [128, 16, 128, 256], P('kv', 'tp'), may hold values from -4 to 4
- mixer_gain: float32 [4096], P('kv'), may hold values from 0.1 to 1.9
- query_weight: bfloat16 [4096, 2048], P('kv', 'tp'), may hold values from -0.09375 to 0.09375
- key_weight: bfloat16 [4096, 2048], P('kv', 'tp'), may hold values from -0.09375 to 0.09375
- value_weight: bfloat16 [4096, 4096], P('kv', 'tp'), may hold values from -0.09375 to 0.09375
- gate_weight: bfloat16 [4096, 4096], P('kv', 'tp'), may hold values from -0.09375 to 0.09375
- output_weight: bfloat16 [4096, 4096], P('tp', 'kv'), may hold values from -0.125 to 0.125
- channel_gain: float32 [4096], P('kv'), may hold values from 0.1 to 1.9
- ffn_gate: bfloat16 [4096, 11264], P('kv', 'tp'), may hold values from -0.09375 to 0.09375
- ffn_up: bfloat16 [4096, 11264], P('kv', 'tp'), may hold values from -0.09375 to 0.09375
- ffn_down: bfloat16 [11264, 4096], P('tp', 'kv'), may hold values from -0.078125 to 0.078125
Outputs:
- layer_output: bfloat16 [128, 4096], P(None, ('kv', 'tp'))
- new_state: float32 [128, 16, 128, 256], P('kv', 'tp')
All inputs are finite; a program needn't handle non-finite values. No bound on the sum of `lengths` on one device may be relied on, other than what follows from the above.
Results may differ from a plain program's by a relative error of at most 0.022.
Values may be sent and summed in bfloat16 or wider, within the bound.
No kernel may reach another device: no remote copies, remote signals or barrier semaphores. Data moves between devices by JAX's collectives and lax.ppermute only.
A program may use at most 64 MiB of HBM per device.

v0:
```python
import jax
import jax.numpy as jnp
from jax import lax
from jax.sharding import PartitionSpec as P

D = 4096
HEADS = 16
QK = 128


def in_blocks(value, dim, devices):
    lengths = value.shape
    blocks = value.reshape(*lengths[:dim], devices, lengths[dim] // devices, *lengths[dim + 1 :])
    return jnp.moveaxis(blocks, dim, 0)


def sent_and_summed(value, axis, dim):
    blocks = in_blocks(value, dim, lax.axis_size(axis))
    arrived = lax.all_to_all(blocks, axis, split_axis=0, concat_axis=0, tiled=True)
    return arrived.astype(jnp.float32).sum(axis=0)


def in_one_piece(arrays, axis, dim, along):
    columns = [a.reshape(*a.shape[:along], -1) for a in arrays]
    both = jnp.concatenate(columns, axis=along)
    result, at, finished = (sent_and_summed(both, axis, dim), 0, [])
    for a, column in zip(arrays, columns):
        piece = result[..., at : at + column.shape[along]]
        finished.append(piece.reshape(*piece.shape[:along], *a.shape[along:]))
        at += column.shape[along]
    return tuple(finished)


def copy_for_each(value, axis):
    devices = lax.axis_size(axis)
    return lax.all_to_all(
        jnp.broadcast_to(value[None], (devices, *value.shape)), axis, 0, 0, tiled=True
    )


def joined_along(blocks, dim):
    blocks = jnp.moveaxis(blocks, 0, dim)
    lengths = blocks.shape
    return blocks.reshape(*lengths[:dim], lengths[dim] * lengths[dim + 1], *lengths[dim + 2 :])


def gather_directly(value, axis, dim):
    blocks = copy_for_each(value, axis)
    return joined_along(blocks, dim)


def rotate_heads(vectors, positions):
    half_dim = vectors.shape[-1] // 2
    frequency = 10000.0 ** (-jnp.arange(half_dim, dtype=jnp.float32) / half_dim)
    angles = positions.astype(jnp.float32)[:, None, None] * frequency
    cosine = jnp.cos(angles)
    sine_part = jnp.sin(angles)
    first_half = vectors[..., :half_dim]
    second = vectors[..., half_dim:]
    return jnp.concatenate(
        [first_half * cosine - second * sine_part, first_half * sine_part + second * cosine],
        axis=-1,
    )


def gathered_rows(columns):
    return lax.all_gather(columns, "tp", axis=1, tiled=True)


def owned_sums(partial_value, squares):
    raw_sums, totals = in_one_piece(
        (partial_value.astype(jnp.bfloat16), squares.astype(jnp.bfloat16)), "kv", 0, 1
    )
    summed = raw_sums * lax.rsqrt(totals / D + 1e-06)[:, None]
    return summed


def on_device(
    tokens,
    lengths,
    retention_state,
    mixer_gain,
    query_weight,
    key_weight,
    value_weight,
    gate_weight,
    output_weight,
    channel_gain,
    ffn_gate,
    ffn_up,
    ffn_down,
):
    feature_block = gathered_rows(tokens).astype(jnp.float32)
    squares = jnp.sum(feature_block * feature_block, axis=1)
    normed = (feature_block * mixer_gain).astype(jnp.bfloat16)
    partial_value = jnp.concatenate(
        [
            jnp.dot(normed, query_weight, preferred_element_type=jnp.float32),
            jnp.dot(normed, key_weight, preferred_element_type=jnp.float32),
            jnp.dot(normed, value_weight, preferred_element_type=jnp.float32),
            jnp.dot(normed, gate_weight, preferred_element_type=jnp.float32),
        ],
        axis=1,
    )
    owned_rows = owned_sums(partial_value, squares)
    local_heads = query_weight.shape[1] // QK
    q_width = query_weight.shape[1]
    v_width = value_weight.shape[1]
    head_width = v_width // local_heads
    seq_rows = owned_rows.shape[0]
    query_rows = rotate_heads(
        owned_rows[:, :q_width].reshape(seq_rows, local_heads, QK), lengths
    ).astype(jnp.bfloat16)
    key_rows = (
        rotate_heads(
            owned_rows[:, q_width : 2 * q_width].reshape(seq_rows, local_heads, QK), lengths
        )
        * QK ** (-0.5)
    ).astype(jnp.bfloat16)
    value_rows = (
        owned_rows[:, 2 * q_width : 2 * q_width + v_width]
        .astype(jnp.bfloat16)
        .reshape(seq_rows, local_heads, head_width)
    )
    gate_rows = owned_rows[:, 2 * q_width + v_width :]
    head_ids = (lax.axis_index("tp") * local_heads + jnp.arange(local_heads)).astype(jnp.float32)
    decay_rate = 1.0 - 2.0 ** (-5.0 - 10.0 * head_ids / (HEADS - 1))
    new_state = (
        decay_rate[None, :, None, None] * retention_state
        + key_rows.astype(jnp.float32)[..., :, None] * value_rows.astype(jnp.float32)[..., None, :]
    )
    retained = jnp.einsum(
        "bhk,bhkv->bhv", query_rows.astype(jnp.float32), new_state, precision=lax.Precision.HIGHEST
    )
    normalized = retained * lax.rsqrt(jnp.mean(retained * retained, axis=-1) + 1e-06)[..., None]
    merged = (normalized.reshape(seq_rows, v_width) * jax.nn.silu(gate_rows)).astype(jnp.bfloat16)
    mixed_part = jnp.dot(
        gather_directly(merged, "kv", 0), output_weight, preferred_element_type=jnp.float32
    )
    mixed_cols = sent_and_summed(mixed_part.astype(jnp.bfloat16), "tp", 1)
    residual = (tokens.astype(jnp.float32) + mixed_cols).astype(jnp.bfloat16)
    block_two = gathered_rows(residual).astype(jnp.float32)
    squares_two = jnp.sum(block_two * block_two, axis=1)
    normed_two = (block_two * channel_gain).astype(jnp.bfloat16)
    partial_two = jnp.concatenate(
        [
            jnp.dot(normed_two, ffn_gate, preferred_element_type=jnp.float32),
            jnp.dot(normed_two, ffn_up, preferred_element_type=jnp.float32),
        ],
        axis=1,
    )
    hidden_units = ffn_gate.shape[1]
    summed = owned_sums(partial_two, squares_two)
    hidden = (jax.nn.silu(summed[:, :hidden_units]) * summed[:, hidden_units:]).astype(jnp.bfloat16)
    down_part = jnp.dot(
        gather_directly(hidden, "kv", 0), ffn_down, preferred_element_type=jnp.float32
    )
    down_sums = sent_and_summed(down_part.astype(jnp.bfloat16), "tp", 1)
    layer_output = (residual.astype(jnp.float32) + down_sums).astype(jnp.bfloat16)
    return (layer_output, new_state)


def solution(mesh):
    in_specs = (
        P(None, ("kv", "tp")),
        P("kv"),
        P("kv", "tp", None, None),
        P("kv"),
        P("kv", "tp"),
        P("kv", "tp"),
        P("kv", "tp"),
        P("kv", "tp"),
        P("tp", "kv"),
        P("kv"),
        P("kv", "tp"),
        P("kv", "tp"),
        P("tp", "kv"),
    )
    out_specs = (P(None, ("kv", "tp")), P("kv", "tp", None, None))
    return jax.shard_map(
        on_device, mesh=mesh, in_specs=in_specs, out_specs=out_specs, check_vma=False
    )
```

profile of v0, /device:TPU:1, one launch (start us, length us, event | category | flops | bytes accessed | tf_op | source)
XLA Modules:
  0.0 126.4 jit_solution(4354620266394448964)
XLA Ops:
  0.6 0.0 copy-start
  0.6 0.0 copy-start.2
  0.7 21.8 %all_gather.6 = bf16[128,256]{0,1:T(8,128)(2,1)S(1)} all-gather(bf16[128,16]{0,1:T(8,128)(2,1)} %param.13), channel_id=1, replica_groups=mesh['kv'=16,'tp'=16] {'tp'}, dimensions={1}, use_global_device_ids=true | all-gather | bytes 69632 | tf_op jit(solution)/shard_map/all_gather | solution.py:67
  22.5 0.1 fusion.12
  22.6 0.2 convert_element_type.141
  22.8 1.8 %fusion.5 = bf16[16,8,769]{2,1,0:T(8,128)(2,1)} fusion(bf16[256,128]{1,0:T(8,128)(2,1)} %param.17, bf16[128,256]{0,1:T(8,128)(2,1)S(1)} %all_gather.6, f32[256]{0:T(256)} %param.16), kind=kOutput, calls=%fused_computation.13 | convolution fusion | flops 8503295 | bytes 164864 | tf_op jit(solution)/shard_map/dot_general | solution.py:98
  24.6 1.8 %fusion.7 = bf16[16,8,769]{2,1,0:T(8,128)(2,1)} fusion(bf16[16,8,769]{2,1,0:T(8,128)(2,1)} %fusion.5, bf16[256,128]{1,0:T(8,128)(2,1)} %param.18, bf16[128,256]{0,1:T(8,128)(2,1)S(1)} %all_gather.6, f32[256]{0:T(256)} %param.16), kind=kOutput, calls=%fused_computation.15 | convolution fusion | flops 8503296 | bytes 164864 | tf_op jit(solution)/shard_map/dot_general | solution.py:99
  26.3 1.8 %fusion.1 = bf16[16,8,769]{2,1,0:T(8,128)(2,1)} fusion(bf16[16,8,769]{2,1,0:T(8,128)(2,1)} %fusion.7, bf16[256,256]{1,0:T(8,128)(2,1)} %param.19, bf16[128,256]{0,1:T(8,128)(2,1)S(1)} %all_gather.6, f32[256]{0:T(256)} %param.16), kind=kOutput, calls=%fused_computation.7 | convolution fusion | flops 16908288 | bytes 263168 | tf_op jit(solution)/shard_map/dot_general | solution.py:100
  28.1 1.8 %fusion.3 = bf16[16,8,769]{2,1,0:T(8,128)(2,1)} fusion(bf16[16,8,769]{2,1,0:T(8,128)(2,1)} %fusion.1, bf16[256,256]{1,0:T(8,128)(2,1)} %param.20, bf16[128,256]{0,1:T(8,128)(2,1)S(1)} %all_gather.6, f32[256]{0:T(256)} %param.16), kind=kOutput, calls=%fused_computation.9 | convolution fusion | flops 16908288 | bytes 263168 | tf_op jit(solution)/shard_map/dot_general | solution.py:101
  30.0 0.6 constant_dynamic-update-slice_fusion
  30.6 6.8 %all-to-all-start = ((bf16[16,8,769]{2,1,0:T(8,128)(2,1)}), bf16[16,8,769]{2,1,0:T(8,128)(2,1)S(1)}, u32[]{:S(2)}, u32[]{:S(2)}) async-start(bf16[16,8,769]{2,1,0:T(8,128)(2,1)} %constant_dynamic-update-slice_fusion), calls=%async_computation | async-start | bytes 458752 | tf_op jit(solution)/shard_map/all_to_all | solution.py:19
  37.4 0.0 copy-start.8
  37.4 0.6 copy-done.8
  38.1 7.3 %all-to-all-done = bf16[16,8,769]{2,1,0:T(8,128)(2,1)S(1)} async-done(((bf16[16,8,769]{2,1,0:T(8,128)(2,1)}), bf16[16,8,769]{2,1,0:T(8,128)(2,1)S(1)}, u32[]{:S(2)}, u32[]{:S(2)}) %all-to-all-start) | async-done | bytes 196896 | tf_op jit(solution)/shard_map/all_to_all | solution.py:19
  45.4 0.1 fusion.44
  45.5 0.1 slice_multiply_fusion.2
  45.6 0.1 fusion.49
  45.7 0.1 maximum_bitcast_fusion
  45.8 0.1 fusion.47
  45.9 0.0 copy-done.2
  45.9 0.2 multiply_add_fusion
  46.1 0.0 copy-start.1
  46.1 0.5 fusion.8
  46.6 0.0 copy-start.5
  46.6 0.1 fusion.19
  46.7 0.1 fusion.21
  46.8 9.2 %all_to_all.30 = bf16[16,8,256]{2,1,0:T(8,128)(2,1)S(1)} all-to-all(bf16[16,8,256]{2,1,0:T(8,128)(2,1)S(1)} %broadcast_in_dim.4), channel_id=1, replica_groups=mesh['kv'=16,'tp'=16] {'kv'}, dimensions={0} | all-to-all | bytes 131072 | tf_op jit(solution)/shard_map/all_to_all | solution.py:36
  55.9 0.0 copy-done.5
  56.0 0.2 convolution_convert_fusion.3
  56.1 0.1 copy.37
  56.2 13.9 %all_to_all.31 = bf16[16,128,16]{1,2,0:T(8,128)(2,1)S(1)} all-to-all(bf16[16,128,16]{1,2,0:T(8,128)(2,1)S(1)} %bitcast.66), channel_id=1, replica_groups=mesh['kv'=16,'tp'=16] {'tp'}, dimensions={0} | all-to-all | bytes 131072 | tf_op jit(solution)/shard_map/all_to_all | solution.py:19
  70.2 0.0 copy-start.6
  70.2 0.7 copy-done.6
  70.9 14.9 %all_gather.7 = bf16[128,256]{0,1:T(8,128)(2,1)S(1)} all-gather(bf16[128,16]{0,1:T(8,128)(2,1)S(1)} %add_convert_fusion.1), channel_id=1, replica_groups=mesh['kv'=16,'tp'=16] {'tp'}, dimensions={1}, use_global_device_ids=true | all-gather | bytes 69632 | tf_op jit(solution)/shard_map/all_gather | solution.py:67
  85.7 0.1 fusion.14
  85.8 0.0 copy-start.7
  85.8 0.2 convert_element_type.142
  86.0 0.0 copy-done
  86.0 0.4 copy-done.7
  86.5 0.0 copy-start.3
  86.5 0.3 convolution_convert_fusion.1
  86.8 0.0 copy-done.1
  86.8 0.1 copy.38
  86.9 0.5 copy-done.3
  87.4 0.3 convolution_convert_fusion
  87.8 0.1 copy.39
  87.9 0.2 concatenate.65
  88.1 12.3 %all_to_all.32 = bf16[16,8,1409]{2,1,0:T(8,128)(2,1)S(1)} all-to-all(bf16[16,8,1409]{2,1,0:T(8,128)(2,1)S(1)} %concatenate.65), channel_id=1, replica_groups=mesh['kv'=16,'tp'=16] {'kv'}, dimensions={0} | all-to-all | bytes 721408 | tf_op jit(solution)/shard_map/all_to_all | solution.py:19
  100.4 0.1 convert_reduce_fusion
  100.5 0.1 fusion.41
  100.6 0.0 copy-start.4
  100.6 0.1 slice_multiply_fusion
  100.7 0.1 fusion.18
  100.8 10.4 %all_to_all.33 = bf16[16,8,704]{2,1,0:T(8,128)(2,1)S(1)} all-to-all(bf16[16,8,704]{2,1,0:T(8,128)(2,1)S(1)} %broadcast_in_dim.5), channel_id=1, replica_groups=mesh['kv'=16,'tp'=16] {'kv'}, dimensions={0} | all-to-all | bytes 360448 | tf_op jit(solution)/shard_map/all_to_all | solution.py:36
  111.1 0.0 copy-done.4
  111.1 0.2 convolution_convert_fusion.2
  111.4 0.1 copy.41
  111.5 14.3 %all_to_all.34 = bf16[16,128,16]{1,2,0:T(8,128)(2,1)S(1)} all-to-all(bf16[16,128,16]{1,2,0:T(8,128)(2,1)S(1)} %bitcast.67), channel_id=1, replica_groups=mesh['kv'=16,'tp'=16] {'tp'}, dimensions={0} | all-to-all | bytes 131072 | tf_op jit(solution)/shard_map/all_to_all | solution.py:19
  125.8 0.6 add_convert_fusion
  (11 shorter events, 0.1 us)
Async XLA Ops:
  0.6 85.4 %copy-start = (bf16[256,704]{0,1:T(8,128)(2,1)S(1)}, bf16[256,704]{0,1:T(8,128)(2,1)}, u32[]{:S(2)}) copy-start(bf16[256,704]{0,1:T(8,128)(2,1)} %param.23) | copy-start | bytes 1081348
  0.6 45.2 %copy-start.2 = (f32[8,1,128,256]{3,2,1,0:T(8,128)S(1)}, f32[8,1,128,256]{3,2,1,0:T(8,128)}, u32[]{:S(2)}) copy-start(f32[8,1,128,256]{3,2,1,0:T(8,128)} %param.15) | copy-start | bytes 3145732
  30.6 14.7 %all-to-all-start = ((bf16[16,8,769]{2,1,0:T(8,128)(2,1)}), bf16[16,8,769]{2,1,0:T(8,128)(2,1)S(1)}, u32[]{:S(2)}, u32[]{:S(2)}) async-start(bf16[16,8,769]{2,1,0:T(8,128)(2,1)} %constant_dynamic-update-slice_fusion), calls=%async_computation | async-start | bytes 458752 | tf_op jit(solution)/shard_map/all_to_all | solution.py:19
  37.4 0.7 copy-start.8
  46.1 40.7 %copy-start.1 = (f32[8,1,128,256]{3,2,1,0:T(8,128)}, f32[8,1,128,256]{3,2,1,0:T(8,128)S(1)}, u32[]{:S(2)}) copy-start(f32[8,1,128,256]{3,2,1,0:T(8,128)S(1)} %multiply_add_fusion) | copy-start | bytes 3145732
  46.6 9.4 %copy-start.5 = (bf16[256,256]{1,0:T(8,128)(2,1)S(1)}, bf16[256,256]{1,0:T(8,128)(2,1)}, u32[]{:S(2)}) copy-start(bf16[256,256]{1,0:T(8,128)(2,1)} %param.21) | copy-start | bytes 393220
  70.2 0.7 copy-start.6
  85.8 0.7 copy-start.7
  86.5 1.0 copy-start.3
  100.6 10.6 %copy-start.4 = (bf16[704,256]{1,0:T(8,128)(2,1)S(1)}, bf16[704,256]{1,0:T(8,128)(2,1)}, u32[]{:S(2)}) copy-start(bf16[704,256]{1,0:T(8,128)(2,1)} %param.25) | copy-start | bytes 1081348
where the time goes:
time: 127 us; the launch traced here: 126 us
  blocking collectives  96.8 us (76%)
  matrix products  8.66 us (7%)
  waiting for transfers between devices  7.25 us (6%)
  starting transfers between devices  6.75 us (5%)
  local copies, waits for them, and re-layouts  4.08 us (3%)
  other arithmetic  1.99 us (2%)
    all_to_all x3, blocking collectives, sent_and_summed(): lax.all_to_all(blocks, axis, split_axis=0, concat_axis=0, tiled=True)  40.5 us
    all_gather x2, blocking collectives, gathered_rows(): return lax.all_gather(columns, 'tp', axis=1, tiled=True)  36.7 us
    all_to_all x2, blocking collectives, copy_for_each(): lax.all_to_all(jnp.broadcast_to(value[None], (devices, *value.shape)), ax...  19.6 us
    all_to_all x1, waiting for transfers between devices, sent_and_summed(): lax.all_to_all(blocks, axis, split_axis=0, concat_axis=0, tiled=True)  7.25 us
    all_to_all x1, starting transfers between devices, sent_and_summed(): lax.all_to_all(blocks, axis, split_axis=0, concat_axis=0, tiled=True)  6.75 us
  transfers between devices with their start and end apart: 1, of which 1 were waited for; matrix products, arithmetic and copies ran while one was open for 0% of the time, Pallas kernels for 0%

commit v1 on v0

--- a/solution.py
+++ b/solution.py
@@ -64,7 +64,12 @@
 
 
 def gathered_rows(columns):
-    return lax.all_gather(columns, "tp", axis=1, tiled=True)
+    return jnp.concatenate(
+        lax.all_to_all(
+            jnp.stack(lax.axis_size("tp") * [columns]), axis_name="tp", split_axis=0, concat_axis=0
+        ),
+        1,
+    )
 
 
 def owned_sums(partial_value, squares):

time: 127 us -> 114 us (0.90)
  blocking collectives: 96.8 us -> 85.4 us
  matrix products: 8.66 us -> 4.5 us
  local copies, waits for them, and re-layouts: 4.08 us -> 6.77 us
    all_gather x2 -> x0, blocking collectives: 36.7 us -> none  [gathered_rows(): return lax.all_gather(columns, 'tp', axis=1, tiled=True)]
    all_to_all x0 -> x2, blocking collectives: none -> 27.9 us  [gathered_rows(): lax.all_to_all(jnp.stack(lax.axis_size('tp') * [columns]), axis_name='tp'...]
    all_to_all x3, blocking collectives: 40.5 us -> 37.9 us  [sent_and_summed(): lax.all_to_all(blocks, axis, split_axis=0, concat_axis=0, tiled=True)]
    convert_element_type x0 -> x4, local copies, waits for them, and re-layouts: none -> 1.85 us  [the longest x2 0.92 us: on_device(): feature_block = gathered_rows(tokens).astype(jnp.float32)]
    unnamed x18 -> x28, local copies, waits for them, and re-layouts: 2.27 us -> 2.66 us
where the time goes in v1:
time: 114 us
  blocking collectives  85.4 us (75%)
  waiting for transfers between devices  7.3 us (6%)
  local copies, waits for them, and re-layouts  6.77 us (6%)
  starting transfers between devices  6.76 us (6%)
  matrix products  4.5 us (4%)
  other arithmetic  2.03 us (2%)
    all_to_all x3, blocking collectives, sent_and_summed(): lax.all_to_all(blocks, axis, split_axis=0, concat_axis=0, tiled=True)  37.9 us
    all_to_all x2, blocking collectives, gathered_rows(): lax.all_to_all(jnp.stack(lax.axis_size('tp') * [columns]), axis_name='tp'...  27.9 us
    all_to_all x2, blocking collectives, copy_for_each(): lax.all_to_all(jnp.broadcast_to(value[None], (devices, *value.shape)), ax...  19.6 us
    all_to_all x1, waiting for transfers between devices, sent_and_summed(): lax.all_to_all(blocks, axis, split_axis=0, concat_axis=0, tiled=True)  7.3 us
    all_to_all x1, starting transfers between devices, sent_and_summed(): lax.all_to_all(blocks, axis, split_axis=0, concat_axis=0, tiled=True)  6.76 us
    unnamed x28, local copies, waits for them, and re-layouts  2.66 us
  transfers between devices with their start and end apart: 1, of which 1 were waited for; matrix products, arithmetic and copies ran while one was open for 0% of the time, Pallas kernels for 0%

profile of v1, /device:TPU:1, one launch (start us, length us, event | category | flops | bytes accessed | tf_op | source)
XLA Modules:
  0.0 113.7 jit_solution(1028293842848873642)
XLA Ops:
  0.6 0.0 copy-start
  0.6 0.7 stack.4
  1.4 17.5 %all_to_all.40 = bf16[16,128,16]{1,2,0:T(8,128)(2,1)S(1)} all-to-all(bf16[16,128,16]{1,2,0:T(8,128)(2,1)S(1)} %stack.4), channel_id=1, replica_groups=mesh['kv'=16,'tp'=16] {'tp'}, dimensions={0} | all-to-all | bytes 131072 | tf_op jit(solution)/shard_map/all_to_all | solution.py:68
  18.9 0.1 fusion.9
  19.0 0.2 convert_element_type.183
  19.2 0.5 copy.39
  19.7 0.0 copy-start.12
  19.7 0.0 copy-start.8
  19.8 0.0 copy-start.9
  19.8 0.0 copy-start.5
  19.8 0.0 copy-start.6
  19.8 0.4 reshape.300
  20.2 0.2 copy-done.12
  20.4 0.2 copy-done.8
  20.6 0.8 fusion.3
  21.4 0.0 copy-done.9
  21.4 0.8 fusion.2
  22.1 0.0 copy-done.5
  22.1 0.8 fusion.1
  22.9 0.0 copy-done.6
  22.9 0.8 fusion
  23.7 0.6 constant_dynamic-update-slice_fusion
  24.4 6.8 %all-to-all-start.1 = ((bf16[16,8,769]{2,1,0:T(8,128)(2,1)}), bf16[16,8,769]{2,1,0:T(8,128)(2,1)S(1)}, u32[]{:S(2)}, u32[]{:S(2)}) async-start(bf16[16,8,769]{2,1,0:T(8,128)(2,1)} %constant_dynamic-update-slice_fusion), calls=%async_computation.1 | async-start | bytes 458752 | tf_op jit(solution)/shard_map/all_to_all | solution.py:19
  31.1 0.0 copy-start.13
  31.1 0.6 copy-done.13
  31.9 7.3 %all-to-all-done.1 = bf16[16,8,769]{2,1,0:T(8,128)(2,1)S(1)} async-done(((bf16[16,8,769]{2,1,0:T(8,128)(2,1)}), bf16[16,8,769]{2,1,0:T(8,128)(2,1)S(1)}, u32[]{:S(2)}, u32[]{:S(2)}) %all-to-all-start.1) | async-done | bytes 196896 | tf_op jit(solution)/shard_map/all_to_all | solution.py:19
  39.2 0.1 fusion.42
  39.3 0.1 slice_multiply_fusion.2
  39.4 0.1 fusion.47
  39.5 0.1 maximum_bitcast_fusion
  39.6 0.1 fusion.45
  39.7 0.0 copy-done.2
  39.7 0.2 multiply_add_fusion
  39.9 0.0 copy-start.1
  39.9 0.5 fusion.4
  40.4 0.1 fusion.17
  40.5 0.1 fusion.19
  40.6 9.2 %all_to_all.41 = bf16[16,8,256]{2,1,0:T(8,128)(2,1)S(1)} all-to-all(bf16[16,8,256]{2,1,0:T(8,128)(2,1)S(1)} %broadcast_in_dim.4), channel_id=1, replica_groups=mesh['kv'=16,'tp'=16] {'kv'}, dimensions={0} | all-to-all | bytes 131072 | tf_op jit(solution)/shard_map/all_to_all | solution.py:36
  49.8 0.0 copy-done.7
  49.8 0.2 convolution_convert_fusion.3
  49.9 0.1 copy.41
  50.1 12.9 %all_to_all.42 = bf16[16,128,16]{1,2,0:T(8,128)(2,1)S(1)} all-to-all(bf16[16,128,16]{1,2,0:T(8,128)(2,1)S(1)} %bitcast.66), channel_id=1, replica_groups=mesh['kv'=16,'tp'=16] {'tp'}, dimensions={0} | all-to-all | bytes 131072 | tf_op jit(solution)/shard_map/all_to_all | solution.py:19
  63.0 0.7 copy-done.10
  63.7 10.4 %all_to_all.43 = bf16[16,128,16]{1,2,0:T(8,128)(2,1)S(1)} all-to-all(bf16[16,128,16]{1,2,0:T(8,128)(2,1)S(1)} %stack.5), channel_id=1, replica_groups=mesh['kv'=16,'tp'=16] {'tp'}, dimensions={0} | all-to-all | bytes 131072 | tf_op jit(solution)/shard_map/all_to_all | solution.py:68
  74.1 0.1 fusion.10
  74.1 0.2 convert_element_type.184
  74.4 0.5 copy.42
  74.9 0.0 copy-start.11
  74.9 0.4 reshape.303
  75.3 0.2 copy-done.11
  75.5 0.3 convolution_convert_fusion
  75.8 0.7 copy-done.4
  76.5 0.3 convolution_convert_fusion.1
  76.8 0.2 concatenate.47
  77.0 12.3 %all_to_all.44 = bf16[16,8,1409]{2,1,0:T(8,128)(2,1)S(1)} all-to-all(bf16[16,8,1409]{2,1,0:T(8,128)(2,1)S(1)} %concatenate.47), channel_id=1, replica_groups=mesh['kv'=16,'tp'=16] {'kv'}, dimensions={0} | all-to-all | bytes 721408 | tf_op jit(solution)/shard_map/all_to_all | solution.py:19
  89.3 0.1 convert_reduce_fusion
  89.3 0.1 fusion.39
  89.5 0.1 slice_multiply_fusion
  89.5 0.1 fusion.16
  89.6 10.4 %all_to_all.45 = bf16[16,8,704]{2,1,0:T(8,128)(2,1)S(1)} all-to-all(bf16[16,8,704]{2,1,0:T(8,128)(2,1)S(1)} %broadcast_in_dim.5), channel_id=1, replica_groups=mesh['kv'=16,'tp'=16] {'kv'}, dimensions={0} | all-to-all | bytes 360448 | tf_op jit(solution)/shard_map/all_to_all | solution.py:36
  100.0 0.2 convolution_convert_fusion.2
  100.2 0.1 copy.44
  100.4 12.7 %all_to_all.46 = bf16[16,128,16]{1,2,0:T(8,128)(2,1)S(1)} all-to-all(bf16[16,128,16]{1,2,0:T(8,128)(2,1)S(1)} %bitcast.67), channel_id=1, replica_groups=mesh['kv'=16,'tp'=16] {'tp'}, dimensions={0} | all-to-all | bytes 131072 | tf_op jit(solution)/shard_map/all_to_all | solution.py:19
  113.1 0.6 add_convert_fusion
  (23 shorter events, 0.2 us)
Async XLA Ops:
  0.6 74.7 %copy-start = (bf16[256,704]{0,1:T(8,128)(2,1)S(1)}, bf16[256,704]{0,1:T(8,128)(2,1)}, u32[]{:S(2)}) copy-start(bf16[256,704]{0,1:T(8,128)(2,1)} %param.24) | copy-start | bytes 1081348
  19.7 0.7 copy-start.12
  19.7 0.8 copy-start.8
  19.8 1.6 %copy-start.9 = (bf16[256,128]{1,0:T(8,128)(2,1)S(1)}, bf16[256,128]{1,0:T(8,128)(2,1)}, u32[]{:S(2)}) copy-start(bf16[256,128]{1,0:T(8,128)(2,1)} %param.18) | copy-start | bytes 196612
  19.8 2.4 %copy-start.5 = (bf16[256,256]{1,0:T(8,128)(2,1)S(1)}, bf16[256,256]{1,0:T(8,128)(2,1)}, u32[]{:S(2)}) copy-start(bf16[256,256]{1,0:T(8,128)(2,1)} %param.19) | copy-start | bytes 393220
  19.8 3.2 %copy-start.6 = (bf16[256,256]{1,0:T(8,128)(2,1)S(1)}, bf16[256,256]{1,0:T(8,128)(2,1)}, u32[]{:S(2)}) copy-start(bf16[256,256]{1,0:T(8,128)(2,1)} %param.20) | copy-start | bytes 393220
  20.4 19.3 %copy-start.2 = (f32[8,1,128,256]{3,2,1,0:T(8,128)S(1)}, f32[8,1,128,256]{3,2,1,0:T(8,128)}, u32[]{:S(2)}) copy-start(f32[8,1,128,256]{3,2,1,0:T(8,128)} %param.15) | copy-start | bytes 3145732
  24.4 14.8 %all-to-all-start.1 = ((bf16[16,8,769]{2,1,0:T(8,128)(2,1)}), bf16[16,8,769]{2,1,0:T(8,128)(2,1)S(1)}, u32[]{:S(2)}, u32[]{:S(2)}) async-start(bf16[16,8,769]{2,1,0:T(8,128)(2,1)} %constant_dynamic-update-slice_fusion), calls=%async_computation.1 | async-start | bytes 458752 | tf_op jit(solution)/shard_map/all_to_all | solution.py:19
  31.1 0.7 copy-start.13
  39.9 34.2 %copy-start.1 = (f32[8,1,128,256]{3,2,1,0:T(8,128)}, f32[8,1,128,256]{3,2,1,0:T(8,128)S(1)}, u32[]{:S(2)}) copy-start(f32[8,1,128,256]{3,2,1,0:T(8,128)S(1)} %multiply_add_fusion) | copy-start | bytes 3145732
  40.4 9.4 %copy-start.7 = (bf16[256,256]{1,0:T(8,128)(2,1)S(1)}, bf16[256,256]{1,0:T(8,128)(2,1)}, u32[]{:S(2)}) copy-start(bf16[256,256]{1,0:T(8,128)(2,1)} %param.21) | copy-start | bytes 393220
  63.0 0.7 copy-start.10
  74.9 0.7 copy-start.11
  75.5 1.0 copy-start.4
  89.5 10.6 %copy-start.3 = (bf16[704,256]{1,0:T(8,128)(2,1)S(1)}, bf16[704,256]{1,0:T(8,128)(2,1)}, u32[]{:S(2)}) copy-start(bf16[704,256]{1,0:T(8,128)(2,1)} %param.25) | copy-start | bytes 1081348
